TPU v7x, 32 devices: a whole 2x2x4 slice. The times are simulated.
32 devices in a mesh: ra: 4 (over z), cb: 2 (over y), dp: 4 (over x, core).
Axes of the slice: x: 2, y: 2, z: 4, core: 2. Of those that a mesh axis runs over, the one named last changes fastest.
Arguments:
- tokens: bfloat16 [1792, 4096], P('dp', 'ra'), may hold values from -70 to 70
- norm_in: bfloat16 [4096], P('ra'), may hold values from 0.099609375 to 1.8984375
- w_up: float32 [4096, 16384], P(None, ('ra', 'cb')), may hold values from -0.09375 to 0.09375
- up_scale: float32 [16384], P(('ra', 'cb')), may hold values from 0.5 to 2
- w_down: float32 [16384, 4096], P('ra', 'cb'), may hold values from -0.0625 to 0.0625
- down_scale: float32 [4096], P('cb'), may hold values from 0.5 to 2
- norm_out: float32 [4096], P('cb'), may hold values from 0.1 to 1.9
Outputs:
- result: bfloat16 [1792, 4096], P('dp', 'cb')
All inputs are finite; a program needn't handle non-finite values.
Results may differ from a plain program's by a relative error of at most 0.024.
Values may be sent and summed in bfloat16 or wider, within the bound.
A program may use at most 128 MiB of HBM per device.

v0:
```python
import functools

import jax
import jax.numpy as jnp
from jax import lax
from jax.experimental import pallas as pl
from jax.experimental.pallas import tpu as pltpu
from jax.sharding import PartitionSpec as P

epsilon = 1e-06
resid_weight = 0.25
MESH = pl.DeviceIdType.MESH
CHUNKS = 4
SLOTS = 6
STEP_ROWS = 128


def plain(tokens, norm_in, w_up, up_scale, w_down, down_scale, norm_out):
    whole_rows, whole_gain = (
        lax.all_gather(tokens, "ra", axis=1, tiled=True),
        lax.all_gather(norm_in, "ra", axis=0, tiled=True),
    )
    whole_float = whole_rows.astype(jnp.float32)
    model_width = whole_float.shape[1]
    inv_in = lax.rsqrt(jnp.mean(whole_float * whole_float, axis=-1) + epsilon)
    normed = (whole_float * whole_gain.astype(jnp.float32)).astype(jnp.bfloat16)
    pre_act = jnp.dot(normed, w_up.astype(jnp.bfloat16), preferred_element_type=jnp.float32)
    pre_act = pre_act * inv_in[:, None] * up_scale
    hidden = jnp.square(jax.nn.relu(pre_act)).astype(jnp.bfloat16)
    down_bf = w_down.astype(jnp.bfloat16)
    quarter = down_bf.shape[1]
    partial_value = jnp.dot(
        lax.all_gather(hidden, "cb", axis=1, tiled=True),
        down_bf,
        preferred_element_type=jnp.float32,
    )
    col_block = lax.axis_index("cb")
    x_quarter = lax.dynamic_slice_in_dim(whole_float, col_block * quarter, quarter, 1)
    down = lax.psum(partial_value.astype(jnp.bfloat16), "ra").astype(jnp.float32)
    mixed = resid_weight * x_quarter + down * down_scale
    total_sq = lax.psum(jnp.sum(mixed * mixed, axis=-1), "cb")
    inv_out = lax.rsqrt(total_sq / model_width + epsilon)
    return (mixed * inv_out[:, None] * norm_out).astype(jnp.bfloat16)


def kernel(
    n, chunks,
    x_ref, gain_ref, wu_ref, us_ref, wd_ref, ds_ref, no_ref,
    o_ref,
    xa, gains, wu, wd, stage, normed, hid, parts, rbuf, down, mixed, sq, sqr,
    load_sem, own_sem, gs, gr,
    xs, xr, ys, yr, hs, hr, rs, rr, fs, fr, qs, qr,
):
    z = lax.axis_index("ra")
    y = lax.axis_index("cb")
    twin = 1 - y
    rows = xa.shape[3]
    half = xa.shape[4]
    model_width = 2 * n * half
    up_cols = wu.shape[1]
    steps = wu.shape[0] // STEP_ROWS

    def load(ref, i, slot):
        return pltpu.make_async_copy(
            ref.at[pl.ds(i * STEP_ROWS, STEP_ROWS)], stage.at[slot], load_sem.at[slot]
        )

    for i in range(SLOTS):
        load(wu_ref, i, i).start()

    def own_piece(c, h):
        return pltpu.make_async_copy(
            x_ref.at[pl.ds(c * rows, rows), pl.ds(h * half, half)],
            xa.at[c, z, h],
            own_sem.at[c, h],
        )

    for c in range(chunks):
        for h in range(2):
            own_piece(c, h).start()

    barrier = pltpu.get_barrier_semaphore()
    for j in range(1, n):
        pl.semaphore_signal(
            barrier, inc=1, device_id={"ra": lax.rem(z + j, n)}, device_id_type=MESH
        )
    pl.semaphore_signal(barrier, inc=1, device_id={"cb": twin}, device_id_type=MESH)
    pl.semaphore_wait(barrier, n)

    def remote(src, dst, send, recv, where):
        return pltpu.make_async_remote_copy(
            src_ref=src, dst_ref=dst, send_sem=send, recv_sem=recv,
            device_id=where, device_id_type=MESH,
        )

    def x_copy(c, src, way):
        piece = xa.at[c, src, y]
        return remote(piece, piece, xs.at[c, src, way], xr.at[c, src], {"ra": z + 1 - 2 * way})

    def y_copy(c, src):
        piece = xa.at[c, src, y]
        return remote(piece, piece, ys.at[c, src], yr.at[c, src], {"cb": twin})

    def y_arrive(c, src):
        piece = xa.at[c, src, twin]
        return remote(piece, piece, ys.at[c, src], yr.at[c, src], {"cb": twin})

    def d_copy(c, src, way):
        piece = down.at[c, src]
        return remote(piece, piece, fs.at[c, src, way], fr.at[c, src], {"ra": z + 1 - 2 * way})

    def start_line(copy, c):
        @pl.when(z + 1 < n)
        def _():
            copy(c, z, 0).start()

        @pl.when(z > 0)
        def _():
            copy(c, z, 1).start()

    def relay(copy, c, k, also=None):
        @pl.when(z - k >= 0)
        def _():
            src = z - k
            copy(c, src, 0).wait_recv()

            @pl.when(z + 1 < n)
            def _():
                copy(c, src, 0).start()

            if also is not None:
                also(c, src).start()

        @pl.when(z + k < n)
        def _():
            src = z + k
            copy(c, src, 1).wait_recv()

            @pl.when(z > 0)
            def _():
                copy(c, src, 1).start()

            if also is not None:
                also(c, src).start()

    def gain_copy(where, src):
        return remote(gain_ref, gains.at[src], gs.at[where], gr.at[src], {"ra": where})

    def begin(c):
        if c < chunks:
            for h in range(2):
                own_piece(c, h).wait()
            start_line(x_copy, c)

    begin(0)
    for j in range(1, n):
        gain_copy(lax.rem(z + j, n), z).start()
    gains[z] = gain_ref[...]
    begin(1)

    def gather_step(c, k):
        relay(x_copy, c, k, y_copy)
        if k == 1:
            begin(c + 2)

    def convert(ref, target, following, lo, hi):
        def body(i, carry):
            slot = lax.rem(i + (0 if following is not None else steps), SLOTS)
            load(ref, i, slot).wait()
            target[pl.ds(pl.multiple_of(i * STEP_ROWS, STEP_ROWS), STEP_ROWS), :] = stage[
                slot
            ].astype(jnp.bfloat16)

            @pl.when(i + SLOTS < steps)
            def _():
                load(ref, i + SLOTS, slot).start()

            if following is not None:
                @pl.when(i + SLOTS >= steps)
                def _():
                    load(following, i + SLOTS - steps, slot).start()

            return carry

        lax.fori_loop(lo, hi, body, 0)

    def convert_with_gather(ref, target, following, among):
        relays = [(c, k) for c in among if c < chunks for k in range(1, n)]
        cuts = [steps * k // (len(relays) + 1) for k in range(len(relays) + 2)]
        for i in range(len(relays) + 1):
            convert(ref, target, following, cuts[i], cuts[i + 1])
            if i < len(relays):
                gather_step(*relays[i])

    def hid_copy(c, block):
        piece = hid.at[c, block]
        return remote(piece, piece, hs.at[c], hr.at[c], {"cb": twin})

    def up(c):
        for j in range(1, n):
            y_arrive(c, lax.rem(z + j, n)).wait_recv()
        total = jnp.zeros((rows, 1), jnp.float32)
        for s in range(n):
            for h in range(2):
                xf = xa[c, s, h].astype(jnp.float32)
                total += jnp.sum(xf * xf, axis=1, keepdims=True)
                gain = gains[s][:, h * half : (h + 1) * half]
                lo = (2 * s + h) * half
                normed[:, lo : lo + half] = (xf * gain).astype(jnp.bfloat16)
        inv_in = lax.rsqrt(total / model_width + epsilon)
        tile = 256

        def body(j, carry):
            cols = pl.ds(pl.multiple_of(j * tile, tile), tile)
            pre = jnp.dot(normed[...], wu[:, cols], preferred_element_type=jnp.float32)
            pre = jnp.maximum(pre * inv_in * us_ref[:, cols], 0.0)
            hid[c, y, :, cols] = (pre * pre).astype(jnp.bfloat16)
            return carry

        lax.fori_loop(0, up_cols // tile, body, 0)
        hid_copy(c, y).start()

    def part_copy(c, where, src):
        return remote(
            parts.at[c, where], rbuf.at[c, src], rs.at[c, where], rr.at[c, src], {"ra": where}
        )

    def down_product(c):
        hid_copy(c, twin).wait_recv()

        def body(q, carry):
            cols = pl.ds(pl.multiple_of(q * half, half), half)
            acc = jnp.dot(hid[c, 0], wd[:up_cols, cols], preferred_element_type=jnp.float32)
            acc += jnp.dot(hid[c, 1], wd[up_cols:, cols], preferred_element_type=jnp.float32)
            parts[c, q] = acc.astype(jnp.bfloat16)
            return carry

        lax.fori_loop(0, n, body, 0)
        for j in range(1, n):
            part_copy(c, lax.rem(z + j, n), z).start()

    def reduce(c):
        acc = parts[c, z].astype(jnp.float32)
        for j in range(1, n):
            src = lax.rem(z + j, n)
            part_copy(c, src, src).wait_recv()
            acc += rbuf[c, src].astype(jnp.float32)
        down[c, z] = acc.astype(jnp.bfloat16)
        start_line(d_copy, c)

    def sq_copy(c):
        return remote(sq.at[c], sqr.at[c], qs.at[c], qr.at[c], {"cb": twin})

    def mix(c):
        total = jnp.zeros((rows, 1), jnp.float32)
        for q in range(n):
            cols = slice(q * half, (q + 1) * half)
            at = y * n + q
            resid = xa[c, at // 2, at % 2].astype(jnp.float32)
            value = resid_weight * resid + down[c, q].astype(jnp.float32) * ds_ref[:, cols]
            mixed[c % 2, :, cols] = value
            total += jnp.sum(value * value, axis=1, keepdims=True)
        sq[c] = jnp.broadcast_to(total, (rows, 128))
        sq_copy(c).start()

    def finish(c):
        sq_copy(c).wait_recv()
        total = sq[c][:, :1] + sqr[c][:, :1]
        inv_out = lax.rsqrt(total / model_width + epsilon)
        o_ref[c * rows : (c + 1) * rows, :] = (mixed[c % 2] * inv_out * no_ref[...]).astype(
            jnp.bfloat16
        )

    convert_with_gather(wu_ref, wu, wd_ref, (0,))
    for j in range(1, n):
        src = lax.rem(z + j, n)
        gain_copy(src, src).wait_recv()
    up(0)
    convert_with_gather(wd_ref, wd, None, (1, 2))
    def spread(c, lo, hi):
        if 0 <= c < chunks:
            for k in range(lo, hi):
                relay(d_copy, c, k)

    for t in range(1, chunks + 4):
        if t < chunks:
            up(t)
        spread(t - 3, 1, 2)
        if 0 <= t - 1 < chunks:
            down_product(t - 1)
        spread(t - 3, 2, n)
        if 2 < t + 2 < chunks:
            for k in range(1, n):
                gather_step(t + 2, k)
        if 0 <= t - 2 < chunks:
            reduce(t - 2)
        if 0 <= t - 4 < chunks:
            finish(t - 4)
        if 0 <= t - 3 < chunks:
            mix(t - 3)

    for j in range(1, n):
        gain_copy(lax.rem(z + j, n), z).wait_send()

    def drain(c, carry):
        for src in range(n):
            @pl.when((src <= z) & (z + 1 < n))
            def _():
                x_copy(c, src, 0).wait_send()
                d_copy(c, src, 0).wait_send()

            @pl.when((src >= z) & (z > 0))
            def _():
                x_copy(c, src, 1).wait_send()
                d_copy(c, src, 1).wait_send()

            @pl.when(z != src)
            def _():
                y_copy(c, src).wait_send()
                part_copy(c, src, z).wait_send()

        hid_copy(c, y).wait_send()
        sq_copy(c).wait_send()
        return carry

    lax.fori_loop(0, chunks, drain, 0)


def fused(n, tokens, norm_in, w_up, up_scale, w_down, down_scale, norm_out):
    chunks = CHUNKS
    rows = tokens.shape[0] // chunks
    half = tokens.shape[1] // 2
    wide = w_down.shape[1]
    bf16, f32 = jnp.bfloat16, jnp.float32
    dma = pltpu.SemaphoreType.DMA
    vmem = pl.BlockSpec(memory_space=pltpu.VMEM)
    far = pl.BlockSpec(memory_space=pl.ANY)
    flops = 2 * tokens.shape[0] * (w_up.size + w_down.size)
    return pl.pallas_call(
        functools.partial(kernel, n, chunks),
        out_shape=jax.ShapeDtypeStruct((tokens.shape[0], wide), bf16),
        in_specs=[far, vmem, far, vmem, far, vmem, vmem],
        out_specs=vmem,
        scratch_shapes=[
            pltpu.VMEM((chunks, n, 2, rows, half), bf16),
            pltpu.VMEM((n, 1, 2 * half), f32),
            pltpu.VMEM(w_up.shape, bf16),
            pltpu.VMEM(w_down.shape, bf16),
            pltpu.VMEM((SLOTS, STEP_ROWS, wide), f32),
            pltpu.VMEM((rows, 2 * half * n), bf16),
            pltpu.VMEM((chunks, 2, rows, w_up.shape[1]), bf16),
            pltpu.VMEM((chunks, n, rows, half), bf16),
            pltpu.VMEM((chunks, n, rows, half), bf16),
            pltpu.VMEM((chunks, n, rows, half), bf16),
            pltpu.VMEM((2, rows, wide), f32),
            pltpu.VMEM((chunks, rows, 128), f32),
            pltpu.VMEM((chunks, rows, 128), f32),
            dma((SLOTS,)),
            dma((chunks, 2)),
            dma((n,)),
            dma((n,)),
            dma((chunks, n, 2)),
            dma((chunks, n)),
            dma((chunks, n)),
            dma((chunks, n)),
            dma((chunks,)),
            dma((chunks,)),
            dma((chunks, n)),
            dma((chunks, n)),
            dma((chunks, n, 2)),
            dma((chunks, n)),
            dma((chunks,)),
            dma((chunks,)),
        ],
        compiler_params=pltpu.CompilerParams(
            collective_id=0, has_side_effects=True, vmem_limit_bytes=67043328
        ),
        cost_estimate=pl.CostEstimate(
            flops=flops, bytes_accessed=4 * (w_up.size + w_down.size), transcendentals=0
        ),
    )(
        tokens,
        norm_in.astype(f32)[None, :],
        w_up,
        up_scale[None, :],
        w_down,
        down_scale[None, :],
        norm_out[None, :],
    )


def solution(mesh):
    n, m = mesh.shape["ra"], mesh.shape["cb"]

    def per_device(tokens, norm_in, w_up, up_scale, w_down, down_scale, norm_out):
        args = (tokens, norm_in, w_up, up_scale, w_down, down_scale, norm_out)
        fits = (
            m == 2
            and n > 1
            and CHUNKS > 1
            and tokens.shape[0] % (CHUNKS * 16) == 0
            and tokens.shape[1] % 256 == 0
            and w_up.shape == w_down.shape
            and w_up.shape[0] % (STEP_ROWS * n) == 0
            and w_up.shape[0] // STEP_ROWS >= SLOTS
            and w_up.shape[1] % 256 == 0
            and w_up.size <= 8 * 1024 * 1024
            and tokens.size * n <= 2 * 1024 * 1024
        )
        return fused(n, *args) if fits else plain(*args)

    placed = (
        P("dp", "ra"),
        P("ra"),
        P(None, ("ra", "cb")),
        P(("ra", "cb")),
        P("ra", "cb"),
        P("cb"),
        P("cb"),
    )
    return jax.shard_map(
        per_device, mesh=mesh, in_specs=placed, out_specs=P("dp", "cb"), check_vma=False
    )
```

profile of v0, /device:TPU:0, one launch (start us, length us, event | category | flops | bytes accessed | tf_op | source)
XLA Modules:
  0.0 144.5 jit_solution(18226311986950524008)
XLA Ops:
  0.0 1.3 broadcast_in_dim.19
  1.3 140.3 %shard_map.73 = bf16[448,2048]{1,0:T(8,128)(2,1)} custom-call(bf16[448,1024]{1,0:T(8,128)(2,1)} %x_ref.1, f32[1,1024]{1,0:T(1,128)} %bitcast.4, f32[4096,2048]{1,0:T(8,128)} %wu_ref.1, f32[1,2048]{1,0:T(1,128)} %bitcast.5, f32[4096,2048]{1,0:T(8,128)} %wd_ref.1, f32[1,2048]{1,0:T(1,128)} %bitcast.6, f32[1,2048]{1,0:T(1,128)} %bitcast.7), custom_call_target="tpu_custom_call" | custom-call | flops 15032385536 | bytes 67108864 | tf_op jit(solution)/shard_map/pallas_call | solution.py:339
  141.6 2.9 %copy.9 = bf16[448,2048]{1,0:T(8,128)(2,1)} copy(bf16[448,2048]{1,0:T(8,128)(2,1)} %shard_map.73) | data formatting | bytes 3670016
where the time goes:
time: 145 us
  Pallas kernels  140 us (97%)
  local copies, waits for them, and re-layouts  2.94 us (2%)
    pallas_call x1, Pallas kernels, fused(): pl.pallas_call(functools.partial(kernel, n, chunks), out_shape=jax.ShapeD...  140 us
    unnamed x1, local copies, waits for them, and re-layouts  2.94 us

commit v1 on v0

v1 whole, which is shorter than its diff:
```python
import functools

import jax
import jax.numpy as jnp
from jax import lax
from jax.experimental import pallas as pl
from jax.experimental.pallas import tpu as pltpu
from jax.sharding import PartitionSpec as P

epsilon = 1e-06
resid_weight = 0.25
MESH = pl.DeviceIdType.MESH
SLOTS = 6
STEP_ROWS = 128
LANES = 128
TILE = 1024
LAG = 2
SHARES = (4, 7, 6, 6, 5)
HALVED = (True, True, True, False, False)


def plain(tokens, norm_in, w_up, up_scale, w_down, down_scale, norm_out):
    whole_rows, whole_gain = (
        lax.all_gather(tokens, "ra", axis=1, tiled=True),
        lax.all_gather(norm_in, "ra", axis=0, tiled=True),
    )
    whole_float = whole_rows.astype(jnp.float32)
    model_width = whole_float.shape[1]
    inv_in = lax.rsqrt(jnp.mean(whole_float * whole_float, axis=-1) + epsilon)
    normed = (whole_float * whole_gain.astype(jnp.float32)).astype(jnp.bfloat16)
    pre_act = jnp.dot(normed, w_up.astype(jnp.bfloat16), preferred_element_type=jnp.float32)
    pre_act = pre_act * inv_in[:, None] * up_scale
    hidden = jnp.square(jax.nn.relu(pre_act)).astype(jnp.bfloat16)
    down_bf = w_down.astype(jnp.bfloat16)
    quarter = down_bf.shape[1]
    partial_value = jnp.dot(
        lax.all_gather(hidden, "cb", axis=1, tiled=True),
        down_bf,
        preferred_element_type=jnp.float32,
    )
    col_block = lax.axis_index("cb")
    x_quarter = lax.dynamic_slice_in_dim(whole_float, col_block * quarter, quarter, 1)
    down = lax.psum(partial_value.astype(jnp.bfloat16), "ra").astype(jnp.float32)
    mixed = resid_weight * x_quarter + down * down_scale
    total_sq = lax.psum(jnp.sum(mixed * mixed, axis=-1), "cb")
    inv_out = lax.rsqrt(total_sq / model_width + epsilon)
    return (mixed * inv_out[:, None] * norm_out).astype(jnp.bfloat16)


def order(n, tiles):
    last = n - 1

    def relays(c, first, stop):
        return [("relay", c, k) for k in range(first, stop)]

    def up(c):
        return [("norm", c)] + [("up", c, j) for j in range(tiles)]

    ops = [("begin", 0), ("gain",), ("begin", 1), ("wu", 0.42), ("relay", 0, 1), ("wu", 0.75)]
    ops += relays(0, 2, last) + [("relay", 1, 1), ("wu", 1.0), ("relay", 0, last), ("begin", 2)]
    ops += relays(1, 2, last) + up(0) + [("relay", 2, 1), ("wd", 0.3), ("relay", 1, last)]
    ops += [("begin", 3), ("wd", 0.55)] + relays(2, 2, last) + [("norm", 1), ("up", 1, 0)]
    ops += [("relay", 2, last)] + [("up", 1, j) for j in range(1, tiles)]
    ops += [("begin", 4), ("relay", 3, 1), ("wd", 0.8)] + relays(3, 2, last) + [("wd", 1.0)]
    ops += [("down", 0)] + up(2) + [("mids", 0), ("relay", 3, last), ("relay", 4, 1)]
    ops += [("down", 1)] + up(3) + relays(4, 2, last) + [("mids", 1), ("relay", 4, last)]
    ops += up(4) + [("down", 2), ("mids", 2), ("down", 3), ("mids", 3), ("down", 4)]
    ops += [("mids", 4)] + [("ends", c) for c in range(5)]
    return ops


def kernel(
    n, plan,
    x_ref, gain_ref, wu_ref, us_ref, wd_ref, ds_ref, no_ref,
    o_ref,
    xa, gains, wu, wd, stage, normed, scale, hid, parts, sums, mixed, lanes, sq, sqr,
    load_sem, own_sem, gs, gr,
    xs, xr, ys, yr, hs, hr, ins, outs, got, qs, qr,
):
    z = lax.axis_index("ra")
    y = lax.axis_index("cb")
    twin = 1 - y
    chunks = len(plan)
    half = xa.shape[3]
    model_width = 2 * n * half
    up_cols = wu.shape[1]
    up_tiles = up_cols // TILE
    steps = wu.shape[0] // STEP_ROWS
    middle = n // 2
    low = z < middle
    inner = jnp.where(low, z + 1, z - 1)
    outer = jnp.where(low, z - 1, z + 1)
    is_mid = (z == middle - 1) | (z == middle)
    has_outer = (z > 0) & (z < n - 1)
    FROM_OUTER, FROM_INNER = 0, 1

    def rows_of(c):
        start, count, _ = plan[c]
        return pl.ds(start, count)

    def load(ref, i, slot):
        return pltpu.make_async_copy(
            ref.at[pl.ds(i * STEP_ROWS, STEP_ROWS)], stage.at[slot], load_sem.at[slot]
        )

    for i in range(SLOTS):
        load(wu_ref, i, i).start()

    def own_piece(c, h):
        return pltpu.make_async_copy(
            x_ref.at[rows_of(c), pl.ds(h * half, half)],
            xa.at[z, h, rows_of(c)],
            own_sem.at[c, h],
        )

    for c in range(chunks):
        for h in range(2):
            own_piece(c, h).start()

    barrier = pltpu.get_barrier_semaphore()
    for j in range(1, n):
        pl.semaphore_signal(
            barrier, inc=1, device_id={"ra": lax.rem(z + j, n)}, device_id_type=MESH
        )
    pl.semaphore_signal(barrier, inc=1, device_id={"cb": twin}, device_id_type=MESH)
    pl.semaphore_wait(barrier, n)

    def remote(src, dst, send, recv, where):
        return pltpu.make_async_remote_copy(
            src_ref=src, dst_ref=dst, send_sem=send, recv_sem=recv,
            device_id=where, device_id_type=MESH,
        )

    def x_copy(c, src, way):
        piece = xa.at[src, y, rows_of(c)] if plan[c][2] else xa.at[src, :, rows_of(c)]
        return remote(piece, piece, xs.at[c, src, way], xr.at[c, src], {"ra": z + 1 - 2 * way})

    def y_copy(c, src):
        piece = xa.at[src, y, rows_of(c)]
        return remote(piece, piece, ys.at[c, src], yr.at[c, src], {"cb": twin})

    def y_arrive(c, src):
        piece = xa.at[src, twin, rows_of(c)]
        return remote(piece, piece, ys.at[c, src], yr.at[c, src], {"cb": twin})

    def start_line(c):
        @pl.when(z + 1 < n)
        def _():
            x_copy(c, z, 0).start()

        @pl.when(z > 0)
        def _():
            x_copy(c, z, 1).start()

    def relay(c, k):
        @pl.when(z - k >= 0)
        def _():
            src = z - k
            x_copy(c, src, 0).wait_recv()

            @pl.when(z + 1 < n)
            def _():
                x_copy(c, src, 0).start()

            if plan[c][2]:
                y_copy(c, src).start()

        @pl.when(z + k < n)
        def _():
            src = z + k
            x_copy(c, src, 1).wait_recv()

            @pl.when(z > 0)
            def _():
                x_copy(c, src, 1).start()

            if plan[c][2]:
                y_copy(c, src).start()

    def gain_copy(where, src):
        return remote(gain_ref, gains.at[src], gs.at[where], gr.at[src], {"ra": where})

    def begin(c):
        for h in range(2):
            own_piece(c, h).wait()
        start_line(c)

    def gain():
        for j in range(1, n):
            gain_copy(lax.rem(z + j, n), z).start()
        gains[z] = gain_ref[...]

    done = {"wu": 0, "wd": 0}

    def convert(name, until):
        ref, target, following = (wu_ref, wu, wd_ref) if name == "wu" else (wd_ref, wd, None)
        first = 0 if following is not None else steps

        def body(i, carry):
            slot = lax.rem(i + first, SLOTS)
            load(ref, i, slot).wait()
            target[pl.ds(pl.multiple_of(i * STEP_ROWS, STEP_ROWS), STEP_ROWS), :] = stage[
                slot
            ].astype(jnp.bfloat16)

            @pl.when(i + SLOTS < steps)
            def _():
                load(ref, i + SLOTS, slot).start()

            if following is not None:
                @pl.when(i + SLOTS >= steps)
                def _():
                    load(following, i + SLOTS - steps, slot).start()

            return carry

        stop = int(steps * until)
        lax.fori_loop(done[name], stop, body, 0)
        done[name] = stop

    def lane_sum(value, total):
        for j in range(value.shape[1] // LANES):
            part = value[:, j * LANES : (j + 1) * LANES]
            total = part if total is None else total + part
        return total

    def hid_copy(c, block, j):
        cols = pl.ds(pl.multiple_of(block * up_cols + j * TILE, TILE), TILE)
        piece = hid.at[rows_of(c), cols]
        return remote(piece, piece, hs.at[c, j], hr.at[c, j], {"cb": twin})

    def norm(c):
        if c == 0:
            for j in range(1, n):
                src = lax.rem(z + j, n)
                gain_copy(src, src).wait_recv()
        if plan[c][2]:
            for j in range(1, n):
                y_arrive(c, lax.rem(z + j, n)).wait_recv()
        rows = plan[c][1]
        total = None
        for s in range(n):
            for h in range(2):
                xf = xa[s, h, rows_of(c)].astype(jnp.float32)
                total = lane_sum(xf * xf, total)
                gain = gains[s][:, h * half : (h + 1) * half]
                lo = (2 * s + h) * half
                normed[:rows, lo : lo + half] = (xf * gain).astype(jnp.bfloat16)
        total = jnp.sum(total, axis=1, keepdims=True)
        inv_in = lax.rsqrt(total / model_width + epsilon)
        scale[:rows] = jnp.broadcast_to(inv_in, (rows, LANES))

    def up(c, j):
        rows = plan[c][1]
        cols = slice(j * TILE, (j + 1) * TILE)
        at = pl.ds(pl.multiple_of(y * up_cols + j * TILE, TILE), TILE)
        pre = jnp.dot(normed[:rows, :], wu[:, cols], preferred_element_type=jnp.float32)
        pre = jnp.maximum(pre * scale[:rows, :1] * us_ref[:, cols], 0.0)
        hid[rows_of(c), at] = (pre * pre).astype(jnp.bfloat16)
        hid_copy(c, y, j).start()

    def inward_copy(c, q, slot):
        return remote(
            parts.at[q, rows_of(c)], sums.at[slot, q, rows_of(c)],
            ins.at[c, q], got.at[c, slot, q], {"ra": inner},
        )

    def send_inward(c, q):
        inward_copy(c, q, jnp.where(is_mid, FROM_INNER, FROM_OUTER)).start()

    def outward_copy(c, q, slot):
        return remote(
            sums.at[slot, q, rows_of(c)], sums.at[FROM_INNER, q, rows_of(c)],
            outs.at[c, q], got.at[c, FROM_INNER, q], {"ra": outer},
        )

    def arrive(c, q, slot):
        piece = sums.at[slot, q, rows_of(c)]
        return remote(piece, piece, ins.at[c, q], got.at[c, slot, q], {"ra": inner})

    def down(c):
        for j in range(up_tiles):
            hid_copy(c, twin, j).wait_recv()
        per = TILE // half

        def body(j, carry):
            cols = pl.ds(pl.multiple_of(j * TILE, TILE), TILE)
            acc = jnp.dot(hid[rows_of(c), :], wd[:, cols], preferred_element_type=jnp.float32)
            for i in range(per):
                q = j * per + i
                parts[q, rows_of(c)] = acc[:, i * half : (i + 1) * half].astype(jnp.bfloat16)

                @pl.when(jnp.logical_not(has_outer))
                def _():
                    send_inward(c, q)

            return carry

        lax.fori_loop(0, n // per, body, 0)

    def inward(c, q):
        arrive(c, q, FROM_OUTER).wait_recv()
        both = parts[q, rows_of(c)].astype(jnp.float32) + sums[
            FROM_OUTER, q, rows_of(c)
        ].astype(jnp.float32)
        parts[q, rows_of(c)] = both.astype(jnp.bfloat16)
        send_inward(c, q)

    def sq_copy(c):
        return remote(sq.at[c], sqr.at[c], qs.at[c], qr.at[c], {"cb": twin})

    def row_blocks(c):
        rows = plan[c][1]
        return [(lo, min(LANES, rows - lo)) for lo in range(0, rows, LANES)]

    def outward(c, q):
        arrive(c, q, FROM_INNER).wait_recv()

        @pl.when(is_mid)
        def _():
            both = parts[q, rows_of(c)].astype(jnp.float32) + sums[
                FROM_INNER, q, rows_of(c)
            ].astype(jnp.float32)
            sums[FROM_OUTER, q, rows_of(c)] = both.astype(jnp.bfloat16)

        slot = jnp.where(is_mid, FROM_OUTER, FROM_INNER)

        @pl.when(has_outer)
        def _():
            outward_copy(c, q, slot).start()

        cols = pl.ds(pl.multiple_of(q * half, half), half)
        at = y * n + q
        resid = xa[lax.div(at, 2), lax.rem(at, 2), rows_of(c)].astype(jnp.float32)
        value = resid_weight * resid + sums[slot, q, rows_of(c)].astype(
            jnp.float32
        ) * ds_ref[:, cols]
        mixed[rows_of(c), cols] = value
        lanes[rows_of(c)] = lane_sum(value * value, lanes[rows_of(c)])

    def send_squares(c):
        rows = plan[c][1]
        total = jnp.sum(lanes[rows_of(c)], axis=1, keepdims=True)
        total = jnp.broadcast_to(total, (rows, LANES))
        for b, (lo, size) in enumerate(row_blocks(c)):
            block = total[lo : lo + size]
            if size < LANES:
                fill = jnp.zeros((LANES - size, LANES), jnp.float32)
                block = jnp.concatenate([block, fill], axis=0)
            sq[c, b] = block.T[:8]
        sq_copy(c).start()

    def clear(c):
        lanes[rows_of(c)] = jnp.zeros((plan[c][1], LANES), jnp.float32)

    def finish(c):
        start, rows, _ = plan[c]
        sq_copy(c).wait_recv()
        for b, (lo, size) in enumerate(row_blocks(c)):
            total = jnp.broadcast_to((sq[c, b] + sqr[c, b])[:1], (LANES, LANES)).T[:size, :1]
            inv_out = lax.rsqrt(total / model_width + epsilon)
            at = pl.ds(start + lo, size)
            o_ref[at, :] = (mixed[at, :] * inv_out * no_ref[...]).astype(jnp.bfloat16)

    def mids(c):
        final = c == chunks - 1

        @pl.when(has_outer)
        def _():
            if c > 0:
                clear(c - 1)
            if final:
                clear(c)

            def body(step, carry):
                inward(c, step)
                if c > 0:
                    outward(c - 1, step)
                if final:
                    @pl.when(step >= LAG)
                    def _():
                        outward(c, step - LAG)

                return carry

            lax.fori_loop(0, n, body, 0)
            if c > 0:
                send_squares(c - 1)
            if c > 1:
                finish(c - 2)
            if final:
                def rest(q, carry):
                    outward(c, q)
                    return carry

                lax.fori_loop(n - LAG, n, rest, 0)
                send_squares(c)
                for done_chunk in range(max(c - 1, 0), chunks):
                    finish(done_chunk)

    def ends(c):
        @pl.when(jnp.logical_not(has_outer))
        def _():
            clear(c)

            def body(q, carry):
                outward(c, q)
                return carry

            lax.fori_loop(0, n, body, 0)
            send_squares(c)
            if c > 0:
                finish(c - 1)
            if c == chunks - 1:
                finish(c)

    table = {
        "begin": begin, "gain": gain, "relay": relay, "up": up, "down": down,
        "norm": norm, "mids": mids, "ends": ends,
        "wu": functools.partial(convert, "wu"), "wd": functools.partial(convert, "wd"),
    }
    for name, *rest in order(n, up_tiles):
        with jax.named_scope("_".join([name] + [str(r) for r in rest])):
            table[name](*rest)

    for j in range(1, n):
        gain_copy(lax.rem(z + j, n), z).wait_send()

    for c in range(chunks):
        for src in range(n):
            @pl.when((src <= z) & (z + 1 < n))
            def _():
                x_copy(c, src, 0).wait_send()

            @pl.when((src >= z) & (z > 0))
            def _():
                x_copy(c, src, 1).wait_send()

            if plan[c][2]:
                @pl.when(z != src)
                def _():
                    y_copy(c, src).wait_send()

        for j in range(up_tiles):
            hid_copy(c, y, j).wait_send()

        for q in range(n):
            inward_copy(c, q, FROM_OUTER).wait_send()

            @pl.when(has_outer)
            def _():
                outward_copy(c, q, FROM_OUTER).wait_send()

        sq_copy(c).wait_send()


def split_rows(total):
    unit, whole = 16, sum(SHARES)
    if total % (unit * whole):
        return None
    plan, start = [], 0
    for share, halved in zip(SHARES, HALVED):
        count = total * share // whole
        plan.append((start, count, halved))
        start += count
    return tuple(plan)


def fused(n, plan, tokens, norm_in, w_up, up_scale, w_down, down_scale, norm_out):
    chunks = len(plan)
    total_rows = tokens.shape[0]
    most = max(count for _, count, _ in plan)
    half = tokens.shape[1] // 2
    wide = w_down.shape[1]
    up_cols = w_up.shape[1]
    blocks = -(-most // LANES)
    bf16, f32 = jnp.bfloat16, jnp.float32
    dma = pltpu.SemaphoreType.DMA
    vmem = pl.BlockSpec(memory_space=pltpu.VMEM)
    far = pl.BlockSpec(memory_space=pl.ANY)
    flops = 2 * tokens.shape[0] * (w_up.size + w_down.size)
    return pl.pallas_call(
        functools.partial(kernel, n, plan),
        out_shape=jax.ShapeDtypeStruct((tokens.shape[0], wide), bf16),
        in_specs=[far, vmem, far, vmem, far, vmem, vmem],
        out_specs=vmem,
        scratch_shapes=[
            pltpu.VMEM((n, 2, total_rows, half), bf16),
            pltpu.VMEM((n, 1, 2 * half), f32),
            pltpu.VMEM(w_up.shape, bf16),
            pltpu.VMEM(w_down.shape, bf16),
            pltpu.VMEM((SLOTS, STEP_ROWS, wide), f32),
            pltpu.VMEM((most, 2 * half * n), bf16),
            pltpu.VMEM((most, LANES), f32),
            pltpu.VMEM((total_rows, 2 * up_cols), bf16),
            pltpu.VMEM((n, total_rows, half), bf16),
            pltpu.VMEM((2, n, total_rows, half), bf16),
            pltpu.VMEM((total_rows, wide), f32),
            pltpu.VMEM((total_rows, LANES), f32),
            pltpu.VMEM((chunks, blocks, 8, LANES), f32),
            pltpu.VMEM((chunks, blocks, 8, LANES), f32),
            dma((SLOTS,)),
            dma((chunks, 2)),
            dma((n,)),
            dma((n,)),
            dma((chunks, n, 2)),
            dma((chunks, n)),
            dma((chunks, n)),
            dma((chunks, n)),
            dma((chunks, up_cols // TILE)),
            dma((chunks, up_cols // TILE)),
            dma((chunks, n)),
            dma((chunks, n)),
            dma((chunks, 2, n)),
            dma((chunks,)),
            dma((chunks,)),
        ],
        compiler_params=pltpu.CompilerParams(
            collective_id=0, has_side_effects=True, vmem_limit_bytes=67043328
        ),
        cost_estimate=pl.CostEstimate(
            flops=flops, bytes_accessed=4 * (w_up.size + w_down.size), transcendentals=0
        ),
    )(
        tokens,
        norm_in.astype(f32)[None, :],
        w_up,
        up_scale[None, :],
        w_down,
        down_scale[None, :],
        norm_out[None, :],
    )


def solution(mesh):
    n, m = mesh.shape["ra"], mesh.shape["cb"]

    def per_device(tokens, norm_in, w_up, up_scale, w_down, down_scale, norm_out):
        args = (tokens, norm_in, w_up, up_scale, w_down, down_scale, norm_out)
        plan = split_rows(tokens.shape[0])
        half = tokens.shape[1] // 2
        fits = (
            m == 2
            and n > 1
            and n % 2 == 0
            and plan is not None
            and tokens.shape[1] % (2 * LANES) == 0
            and TILE % half == 0
            and w_up.shape == w_down.shape
            and w_down.shape[1] == n * half
            and w_up.shape[0] == 2 * n * half
            and w_up.shape[0] % (STEP_ROWS * n) == 0
            and w_up.shape[0] // STEP_ROWS >= SLOTS
            and w_up.shape[1] % TILE == 0
            and w_up.size <= 8 * 1024 * 1024
            and tokens.size * n <= 2 * 1024 * 1024
        )
        return fused(n, plan, *args) if fits else plain(*args)

    placed = (
        P("dp", "ra"),
        P("ra"),
        P(None, ("ra", "cb")),
        P(("ra", "cb")),
        P("ra", "cb"),
        P("cb"),
        P("cb"),
    )
    return jax.shard_map(
        per_device, mesh=mesh, in_specs=placed, out_specs=P("dp", "cb"), check_vma=False
    )
```

time: 145 us -> 111 us (0.77)
  Pallas kernels: 140 us -> 106 us
    pallas_call x1, Pallas kernels: 140 us -> 106 us  [fused(): pl.pallas_call(functools.partial(kernel, n, plan), out_shape=jax.ShapeDty...]
where the time goes in v1:
time: 111 us; the launch traced here: 110 us
  Pallas kernels  106 us (95%)
  local copies, waits for them, and re-layouts  2.94 us (3%)
  other arithmetic  1.27 us (1%)
    pallas_call x1, Pallas kernels, fused(): pl.pallas_call(functools.partial(kernel, n, plan), out_shape=jax.ShapeDty...  106 us
    unnamed x1, local copies, waits for them, and re-layouts  2.94 us

profile of v1, /device:TPU:0, one launch (start us, length us, event | category | flops | bytes accessed | tf_op | source)
XLA Modules:
  0.0 110.4 jit_solution(4042722998647943866)
XLA Ops:
  0.0 1.3 %broadcast_in_dim.19 = f32[1024]{0:T(1024)} convert(bf16[1024]{0:T(1024)(128)(2,1)} %param.8) | non-fusion elementwise | flops 1024 | bytes 6144 | tf_op jit(solution)/shard_map/broadcast_in_dim | solution.py:526
  1.3 106.2 %shard_map.73 = bf16[448,2048]{1,0:T(8,128)(2,1)} custom-call(bf16[448,1024]{1,0:T(8,128)(2,1)} %x_ref.1, f32[1,1024]{1,0:T(1,128)} %bitcast.4, f32[4096,2048]{1,0:T(8,128)} %wu_ref.1, f32[1,2048]{1,0:T(1,128)} %bitcast.5, f32[4096,2048]{1,0:T(8,128)} %wd_ref.1, f32[1,2048]{1,0:T(1,128)} %bitcast.6, f32[1,2048]{1,0:T(1,128)} %bitcast.7), custom_call_target="tpu_custom_call" | custom-call | flops 15032385536 | bytes 67108864 | tf_op jit(solution)/shard_map/pallas_call | solution.py:482
  107.5 2.9 %copy.9 = bf16[448,2048]{1,0:T(8,128)(2,1)} copy(bf16[448,2048]{1,0:T(8,128)(2,1)} %shard_map.73) | data formatting | bytes 3670016

commit v2 on v1

--- a/solution.py
+++ b/solution.py
@@ -15,7 +15,7 @@
 LANES = 128
 TILE = 1024
 LAG = 2
-SHARES = (4, 7, 6, 6, 5)
+SHARES = (4, 7, 7, 6, 4)
 HALVED = (True, True, True, False, False)
 
 
@@ -58,14 +58,14 @@
 
     ops = [("begin", 0), ("gain",), ("begin", 1), ("wu", 0.42), ("relay", 0, 1), ("wu", 0.75)]
     ops += relays(0, 2, last) + [("relay", 1, 1), ("wu", 1.0), ("relay", 0, last), ("begin", 2)]
-    ops += relays(1, 2, last) + up(0) + [("relay", 2, 1), ("wd", 0.3), ("relay", 1, last)]
-    ops += [("begin", 3), ("wd", 0.55)] + relays(2, 2, last) + [("norm", 1), ("up", 1, 0)]
-    ops += [("relay", 2, last)] + [("up", 1, j) for j in range(1, tiles)]
-    ops += [("begin", 4), ("relay", 3, 1), ("wd", 0.8)] + relays(3, 2, last) + [("wd", 1.0)]
-    ops += [("down", 0)] + up(2) + [("mids", 0), ("relay", 3, last), ("relay", 4, 1)]
-    ops += [("down", 1)] + up(3) + relays(4, 2, last) + [("mids", 1), ("relay", 4, last)]
-    ops += up(4) + [("down", 2), ("mids", 2), ("down", 3), ("mids", 3), ("down", 4)]
-    ops += [("mids", 4)] + [("ends", c) for c in range(5)]
+    ops += relays(1, 2, last) + up(0) + [("relay", 2, 1), ("wd", 0.25), ("relay", 1, last)]
+    ops += [("begin", 3), ("wd", 0.5)] + relays(2, 2, last) + [("wd", 0.75), ("relay", 2, last)]
+    ops += [("begin", 4), ("wd", 1.0)] + up(1) + [("relay", 3, 1), ("down", 0)]
+    ops += relays(3, 2, last) + [("relay", 4, 1)] + up(2) + [("mids", 0)]
+    ops += relays(4, 2, last) + [("relay", 3, last), ("tail", 0), ("down", 1)] + up(3)
+    ops += [("relay", 4, last)] + up(4) + [("mids", 1), ("down", 2), ("tail", 1)]
+    ops += [("mids", 2), ("down", 3), ("tail", 2), ("mids", 3), ("down", 4), ("tail", 3)]
+    ops += [("mids", 4), ("tail", 4)] + [("ends", c) for c in range(5)]
     return ops
 
 
@@ -243,9 +243,14 @@
             for h in range(2):
                 xf = xa[s, h, rows_of(c)].astype(jnp.float32)
                 total = lane_sum(xf * xf, total)
-                gain = gains[s][:, h * half : (h + 1) * half]
+                gain = gains[s].astype(jnp.float32)
                 lo = (2 * s + h) * half
-                normed[:rows, lo : lo + half] = (xf * gain).astype(jnp.bfloat16)
+                for j in range(half // LANES):
+                    at = h * (half // LANES) + j
+                    part = xf[:, j * LANES : (j + 1) * LANES] * gain[at : at + 1]
+                    normed[:rows, lo + j * LANES : lo + (j + 1) * LANES] = part.astype(
+                        jnp.bfloat16
+                    )
         total = jnp.sum(total, axis=1, keepdims=True)
         inv_in = lax.rsqrt(total / model_width + epsilon)
         scale[:rows] = jnp.broadcast_to(inv_in, (rows, LANES))
@@ -363,40 +368,34 @@
             o_ref[at, :] = (mixed[at, :] * inv_out * no_ref[...]).astype(jnp.bfloat16)
 
     def mids(c):
-        final = c == chunks - 1
-
         @pl.when(has_outer)
         def _():
-            if c > 0:
-                clear(c - 1)
-            if final:
-                clear(c)
+            clear(c)
 
             def body(step, carry):
                 inward(c, step)
-                if c > 0:
-                    outward(c - 1, step)
-                if final:
-                    @pl.when(step >= LAG)
-                    def _():
-                        outward(c, step - LAG)
+
+                @pl.when(step >= LAG)
+                def _():
+                    outward(c, step - LAG)
 
                 return carry
 
             lax.fori_loop(0, n, body, 0)
+
+    def tail(c):
+        @pl.when(has_outer)
+        def _():
+            def body(q, carry):
+                outward(c, q)
+                return carry
+
+            lax.fori_loop(n - LAG, n, body, 0)
+            send_squares(c)
             if c > 0:
-                send_squares(c - 1)
-            if c > 1:
-                finish(c - 2)
-            if final:
-                def rest(q, carry):
-                    outward(c, q)
-                    return carry
-
-                lax.fori_loop(n - LAG, n, rest, 0)
-                send_squares(c)
-                for done_chunk in range(max(c - 1, 0), chunks):
-                    finish(done_chunk)
+                finish(c - 1)
+            if c == chunks - 1:
+                finish(c)
 
     def ends(c):
         @pl.when(jnp.logical_not(has_outer))
@@ -416,7 +415,7 @@
 
     table = {
         "begin": begin, "gain": gain, "relay": relay, "up": up, "down": down,
-        "norm": norm, "mids": mids, "ends": ends,
+        "norm": norm, "mids": mids, "tail": tail, "ends": ends,
         "wu": functools.partial(convert, "wu"), "wd": functools.partial(convert, "wd"),
     }
     for name, *rest in order(n, up_tiles):
@@ -486,7 +485,7 @@
         out_specs=vmem,
         scratch_shapes=[
             pltpu.VMEM((n, 2, total_rows, half), bf16),
-            pltpu.VMEM((n, 1, 2 * half), f32),
+            pltpu.VMEM((n, 2 * half // LANES, LANES), bf16),
             pltpu.VMEM(w_up.shape, bf16),
             pltpu.VMEM(w_down.shape, bf16),
             pltpu.VMEM((SLOTS, STEP_ROWS, wide), f32),
@@ -523,7 +522,7 @@
         ),
     )(
         tokens,
-        norm_in.astype(f32)[None, :],
+        norm_in.reshape(-1, LANES),
         w_up,
         up_scale[None, :],
         w_down,

time: 111 us -> 107 us (0.964)
  Pallas kernels: 106 us -> 104 us
  other arithmetic: 1.27 us -> 0 us
    pallas_call x1, Pallas kernels: 106 us -> 104 us  [fused(): pl.pallas_call(functools.partial(kernel, n, plan), out_shape=jax.ShapeDty...]
    broadcast_in_dim x1 -> x0, other arithmetic: 1.27 us -> none  [fused(): norm_in.astype(f32)[None, :]]
where the time goes in v2:
time: 107 us
  Pallas kernels  104 us (97%)
  local copies, waits for them, and re-layouts  2.94 us (3%)
    pallas_call x1, Pallas kernels, fused(): pl.pallas_call(functools.partial(kernel, n, plan), out_shape=jax.ShapeDty...  104 us
    unnamed x1, local copies, waits for them, and re-layouts  2.94 us

profile of v2, /device:TPU:0, one launch (start us, length us, event | category | flops | bytes accessed | tf_op | source)
XLA Modules:
  0.0 107.2 jit_solution(1451750110348989519)
XLA Ops:
  0.0 104.3 %shard_map.73 = bf16[448,2048]{1,0:T(8,128)(2,1)} custom-call(bf16[448,1024]{1,0:T(8,128)(2,1)} %x_ref.1, bf16[8,128]{1,0:T(8,128)(2,1)} %bitcast.7, f32[4096,2048]{1,0:T(8,128)} %wu_ref.1, f32[1,2048]{1,0:T(1,128)} %bitcast.4, f32[4096,2048]{1,0:T(8,128)} %wd_ref.1, f32[1,2048]{1,0:T(1,128)} %bitcast.5, f32[1,2048]{1,0:T(1,128)} %bitcast.6), custom_call_target="tpu_custom_call" | custom-call | flops 15032385536 | bytes 67108864 | tf_op jit(solution)/shard_map/pallas_call | solution.py:481
  104.3 2.9 %copy.9 = bf16[448,2048]{1,0:T(8,128)(2,1)} copy(bf16[448,2048]{1,0:T(8,128)(2,1)} %shard_map.73) | data formatting | bytes 3670016
